TPU v7x, 32 devices: a whole 2x2x4 slice. The times are simulated.
32 devices in a mesh: fs: 8 (over z, core), tp: 4 (over y, x).
Axes of the slice: x: 2, y: 2, z: 4, core: 2. Of those that a mesh axis runs over, the one named last changes fastest.
Arguments:
- tokens: bfloat16 [4096, 2048], P('fs'), may hold values from -6 to 6
- cotangent: bfloat16 [4096, 2048], P('fs'), may hold values from -6 to 6
- gate_weight: bfloat16 [2048, 2816], P('fs', 'tp'), may hold values from -0.125 to 0.125
- up_weight: bfloat16 [2048, 2816], P('fs', 'tp'), may hold values from -0.125 to 0.125
- down_weight: bfloat16 [2048, 2816], P('fs', 'tp'), may hold values from -0.109375 to 0.109375
Outputs:
- input_grad: bfloat16 [4096, 2048], P('fs', 'tp')
- gate_grad: float32 [2048, 2816], P('fs', 'tp')
- up_grad: float32 [2048, 2816], P('fs', 'tp')
- down_grad: float32 [2048, 2816], P('fs', 'tp')
All inputs are finite; a program needn't handle non-finite values.
Results may differ from a plain program's by a relative error of at most 0.014.
Values may be sent and summed in bfloat16 or wider, within the bound.
A program may use at most 64 MiB of HBM per device.

v0:
```python
import functools

import jax
import jax.numpy as jnp
from jax import lax
from jax.experimental import pallas as pl
from jax.experimental.pallas import tpu as pltpu
from jax.sharding import PartitionSpec as P


def row_product(left, right):
    return lax.dot_general(
        left, right, (((1,), (1,)), ((), ())), preferred_element_type=jnp.float32
    )


def token_product(left, right):
    return lax.dot_general(
        left, right, (((0,), (0,)), ((), ())), preferred_element_type=jnp.float32
    )


def owner_sum(received, groups):
    return received.reshape(groups, received.shape[0] // groups, received.shape[1]).sum(axis=0)


def plain_shards(tokens, cotangent, gate_weight, up_weight, down_weight):
    groups = lax.axis_size("fs")
    whole_gate, whole_up, whole_down = (
        lax.all_gather(gate_weight, "fs", axis=0, tiled=True),
        lax.all_gather(up_weight, "fs", axis=0, tiled=True),
        lax.all_gather(down_weight, "fs", axis=0, tiled=True),
    )
    gate = jnp.dot(tokens, whole_gate, preferred_element_type=jnp.float32)
    up = jnp.dot(tokens, whole_up, preferred_element_type=jnp.float32)
    hidden_grad = jnp.dot(cotangent, whole_down, preferred_element_type=jnp.float32)
    sig = jax.nn.sigmoid(gate)
    act = gate * sig
    hidden = (act * up).astype(jnp.bfloat16)
    gate_cot = (hidden_grad * up * sig * (1.0 + gate * (1.0 - sig))).astype(jnp.bfloat16)
    up_cot = (hidden_grad * act).astype(jnp.bfloat16)
    partial_value = row_product(gate_cot, whole_gate) + row_product(up_cot, whole_up)
    input_grad = lax.psum_scatter(
        partial_value.astype(jnp.bfloat16), "tp", scatter_dimension=1, tiled=True
    )
    gate_term = token_product(tokens, gate_cot)
    gate_grad = owner_sum(
        lax.all_to_all(
            gate_term.astype(jnp.bfloat16), "fs", split_axis=0, concat_axis=0, tiled=True
        ).astype(gate_term.dtype),
        groups,
    )
    up_term = token_product(tokens, up_cot)
    up_grad = owner_sum(
        lax.all_to_all(
            up_term.astype(jnp.bfloat16), "fs", split_axis=0, concat_axis=0, tiled=True
        ).astype(up_term.dtype),
        groups,
    )
    down_term = token_product(cotangent, hidden)
    down_grad = owner_sum(
        lax.all_to_all(
            down_term.astype(jnp.bfloat16), "fs", split_axis=0, concat_axis=0, tiled=True
        ).astype(down_term.dtype),
        groups,
    )
    return (input_grad, gate_grad, up_grad, down_grad)


MESH = pl.DeviceIdType.MESH
LAG = 2
GATE, UP, DOWN = 0, 1, 2
RIGHT, LEFT, SIBLING = 0, 1, 2


def kernel(
    n, n_tp, parts, tok, cot, gw, uw, dw, ig_out, gate_out, up_out, down_out,
    x, w_all, acc, cots, own_sum, sib_out, sib_in, line_out, line_in, total, ig_part, ig_in,
    local_sem, ag_send, ag_recv, sib_send, sib_recv, line_send, line_recv, ig_send, ig_recv,
):
    me, tp = lax.axis_index("fs"), lax.axis_index("tp")
    z, c = me // 2, me % 2
    nz = n // 2
    other = 2 * z + 1 - c
    rows = gw.shape[1]
    height = gw.shape[0] // parts
    own_columns = ig_out.shape[1]
    pieces = own_columns // rows
    has_left, has_right = z > 0, z < nz - 1
    is_end = jnp.logical_or(z == 0, z == nz - 1)

    def weight_load(t):
        piece = pl.ds((t // 3) * height, height)
        return pltpu.make_async_copy(
            (gw, uw, dw)[t % 3].at[piece, :], w_all.at[t, me], local_sem.at[t]
        )

    loads = [weight_load(t) for t in range(3 * parts)]
    loads += [
        pltpu.make_async_copy(tok, x.at[0], local_sem.at[3 * parts]),
        pltpu.make_async_copy(cot, x.at[1], local_sem.at[3 * parts + 1]),
    ]
    for load in loads:
        load.start()

    barrier = pltpu.get_barrier_semaphore()
    pl.semaphore_signal(barrier, inc=1, device_id={"fs": other}, device_id_type=MESH)
    for step in range(1, n_tp):
        pl.semaphore_signal(
            barrier, inc=1, device_id={"tp": lax.rem(tp + step, n_tp)}, device_id_type=MESH
        )

    @pl.when(has_right)
    def _():
        pl.semaphore_signal(barrier, inc=1, device_id={"fs": me + 2}, device_id_type=MESH)

    @pl.when(has_left)
    def _():
        pl.semaphore_signal(barrier, inc=1, device_id={"fs": me - 2}, device_id_type=MESH)

    pl.semaphore_wait(barrier, n_tp + has_left.astype(jnp.int32) + has_right.astype(jnp.int32))

    def gather_copy(w, chip, way):
        slot = 2 * chip + c
        device = (me + 2, me - 2, other)[way]
        return pltpu.make_async_remote_copy(
            src_ref=w_all.at[w, slot], dst_ref=w_all.at[w, slot],
            send_sem=ag_send.at[w, way, chip], recv_sem=ag_recv.at[w, slot],
            device_id={"fs": device}, device_id_type=MESH,
        )

    def gather_wait(w, slot):
        pltpu.make_async_remote_copy(
            src_ref=w_all.at[w, slot], dst_ref=w_all.at[w, slot],
            send_sem=ag_send.at[w, SIBLING, 0], recv_sem=ag_recv.at[w, slot],
            device_id={"fs": other}, device_id_type=MESH,
        ).wait_recv()

    for t in range(3 * parts):
        loads[t].wait()

        @pl.when(jnp.logical_and(has_right, jnp.logical_or(z == 0, t == 0)))
        def _():
            gather_copy(t, z, RIGHT).start()

        @pl.when(jnp.logical_and(has_left, jnp.logical_or(z == nz - 1, t == 0)))
        def _():
            gather_copy(t, z, LEFT).start()

        gather_copy(t, z, SIBLING).start()
    loads[3 * parts].wait()
    loads[3 * parts + 1].wait()

    def gather_step(w, s):
        @pl.when(jnp.logical_and(s > 0, z - s >= 0))
        def _():
            gather_wait(w, me - 2 * s)

            @pl.when(has_right)
            def _():
                gather_copy(w, z - s, RIGHT).start()

            gather_copy(w, z - s, SIBLING).start()

        @pl.when(jnp.logical_and(s > 0, z + s < nz))
        def _():
            gather_wait(w, me + 2 * s)

            @pl.when(has_left)
            def _():
                gather_copy(w, z + s, LEFT).start()

            gather_copy(w, z + s, SIBLING).start()

        more = jnp.logical_and(w < 3 * parts - 1, jnp.logical_not(is_end))

        @pl.when(jnp.logical_and(more, s == z))
        def _():
            gather_copy(w + 1, z, RIGHT).start()

        @pl.when(jnp.logical_and(more, s == nz - 1 - z))
        def _():
            gather_copy(w + 1, z, LEFT).start()

        def block(j, carry):
            way, core = j % 2, j // 2
            chip = z + s * (2 * way - 1)
            here = jnp.logical_and(jnp.logical_and(chip >= 0, chip < nz), way * 1 <= s)
            slot = 2 * chip + core * (1 - c) + (1 - core) * c

            @pl.when(here)
            def _():
                @pl.when(core == 1)
                def _():
                    gather_wait(w, slot)

                columns = pl.ds(pl.multiple_of(slot * rows, rows), rows)
                kind = w % 3
                acc[kind] += row_product(w_all[w, slot], x[kind // 2, :, columns])

            return carry

        lax.fori_loop(0, 4, block, 0)

    def gather(w):
        def body(s, carry):
            gather_step(w, s)
            return carry

        lax.fori_loop(0, nz, body, 0)

    def by_rows(body):
        strip = 16

        def step(i, carry):
            body(pl.ds(pl.multiple_of(i * strip, strip), strip))
            return carry

        lax.fori_loop(0, height // strip, step, 0)

    def term(g, slot):
        columns = pl.ds(pl.multiple_of(slot * rows, rows), rows)
        return jnp.dot(
            cots[g], x[(g % 3) // 2, :, columns], preferred_element_type=jnp.float32
        )

    def sibling_copy(g, chip):
        return pltpu.make_async_remote_copy(
            src_ref=sib_out.at[g, chip], dst_ref=sib_in.at[g, chip],
            send_sem=sib_send.at[g, chip], recv_sem=sib_recv.at[g, chip],
            device_id={"fs": other}, device_id_type=MESH,
        )

    def line_copy(g, way, chip):
        return pltpu.make_async_remote_copy(
            src_ref=line_out.at[g, chip], dst_ref=line_in.at[g, way, chip],
            send_sem=line_send.at[g, chip], recv_sem=line_recv.at[g, way, chip],
            device_id={"fs": me + 2 - 4 * way}, device_id_type=MESH,
        )

    def sibling_term(g, chip):
        sib_out[g, chip] = term(g, 2 * chip + 1 - c).astype(jnp.bfloat16)
        sibling_copy(g, chip).start()

    def pair_sum(g, chip):
        own = term(g, 2 * chip + c)
        sibling_copy(g, chip).wait_recv()
        return own + sib_in[g, chip].astype(jnp.float32)

    def each_way(k, body):
        def one(j, carry):
            way = jnp.where(z * 2 >= nz, 1 - j, j)
            chip = jnp.where(way == RIGHT, nz - k, k - 1)
            active = jnp.where(way == RIGHT, chip - z, z - chip) > 0

            @pl.when(active)
            def _():
                body(way, chip)

            return carry

        lax.fori_loop(0, 2, one, 0)

    def sibling_terms(g):
        def body(k, carry):
            each_way(k, lambda way, chip: sibling_term(g, chip))
            return carry

        lax.fori_loop(1, nz, body, 0)
        sibling_term(g, z)

    def reduce_step(g, k):
        def one(way, chip):
            behind = jnp.where(way == RIGHT, z, nz - 1 - z) > 0
            total[...] = pair_sum(g, chip)

            @pl.when(behind)
            def _():
                line_copy(g, way, chip).wait_recv()
                total[...] += line_in[g, way, chip].astype(jnp.float32)

            line_out[g, chip] = total[...].astype(jnp.bfloat16)
            line_copy(g, way, chip).start()

        each_way(k, one)

    def reduce_own(g):
        own_sum[g] = pair_sum(g, z)

    def reduce_final(g):
        @pl.when(has_left)
        def _():
            line_copy(g, RIGHT, z).wait_recv()
            own_sum[g] += line_in[g, RIGHT, z].astype(jnp.float32)

        @pl.when(has_right)
        def _():
            line_copy(g, LEFT, z).wait_recv()
            own_sum[g] += line_in[g, LEFT, z].astype(jnp.float32)

        piece = pl.ds((g // 3) * height, height)
        (gate_out, up_out, down_out)[g % 3][piece, :] = own_sum[g]

    def reduce_all(g, now):
        @pl.when(now)
        def _():
            sibling_terms(g)

            def body(k, carry):
                reduce_step(g, k)
                return carry

            lax.fori_loop(1, nz, body, 0)
            reduce_own(g)

    def input_copy(peer, source):
        return pltpu.make_async_remote_copy(
            src_ref=ig_part.at[peer], dst_ref=ig_in.at[source],
            send_sem=ig_send.at[peer], recv_sem=ig_recv.at[source],
            device_id={"tp": peer}, device_id_type=MESH,
        )

    def input_part(step):
        peer = lax.rem(tp + 1 + step, n_tp)

        def piece(i, carry):
            slot = peer * pieces + i
            value = token_product(cots[GATE], w_all[GATE, slot])
            for t in [t for t in range(1, 3 * parts) if t % 3 != DOWN]:
                value = value + token_product(cots[t], w_all[t, slot])
            ig_part[peer, :, pl.ds(pl.multiple_of(i * rows, rows), rows)] = value.astype(jnp.bfloat16)
            return carry

        lax.fori_loop(0, pieces, piece, 0)

        @pl.when(step < n_tp - 1)
        def _():
            input_copy(peer, tp).start()

    def make_hidden(t):
        def strip(r):
            gate = acc[GATE, r, :]
            sig = jax.nn.sigmoid(gate)
            act = gate * sig
            up = acc[UP, r, :]
            cots[t + 1, r, :] = (act * up).astype(jnp.bfloat16)
            acc[UP, r, :] = up * sig * (1.0 + gate * (1.0 - sig))
            acc[GATE, r, :] = act

        by_rows(strip)

    def make_cots(t):
        def strip(r):
            hidden_grad = acc[DOWN, r, :]
            cots[t - 2, r, :] = (hidden_grad * acc[UP, r, :]).astype(jnp.bfloat16)
            cots[t - 1, r, :] = (hidden_grad * acc[GATE, r, :]).astype(jnp.bfloat16)

        by_rows(strip)

    def in_turn(i):
        return 3 * (i // 3) + (i + 2) % 3

    def gather_and_reduce(t, carry):
        kind = t % 3
        g = jnp.where(kind == DOWN, t, t - 3)
        acc[kind] = jnp.zeros(acc.shape[1:], acc.dtype)
        reduce_all(g, jnp.logical_and(g >= 0, is_end))
        gather(t)
        turn = t - 2 - LAG
        reduce_all(in_turn(turn), jnp.logical_and(turn >= 0, jnp.logical_not(is_end)))

        @pl.when(kind == UP)
        def _():
            make_hidden(t)

        @pl.when(kind == DOWN)
        def _():
            make_cots(t)

        return carry

    lax.fori_loop(0, 3 * parts, gather_and_reduce, 0)
    last = 3 * parts - 3

    def catch_up(turn, carry):
        reduce_all(in_turn(turn), jnp.logical_not(is_end))
        return carry

    lax.fori_loop(max(3 * parts - 2 - LAG, 0), 3 * parts - 2, catch_up, 0)
    steps = max(nz - 1, 1)

    def last_two(i, carry):
        g = last + i // steps

        @pl.when(jnp.logical_and(i < 2 * steps, i % steps == 0))
        def _():
            sibling_terms(g)

        @pl.when(jnp.logical_and(i < n_tp, jnp.logical_not(is_end)))
        def _():
            input_part(i)

        @pl.when(i < 2 * (nz - 1))
        def _():
            reduce_step(g, i % steps + 1)

        @pl.when(jnp.logical_and(i < n_tp, is_end))
        def _():
            input_part(i)

        return carry

    lax.fori_loop(0, max(2 * steps, n_tp), last_two, 0)
    reduce_own(last)
    reduce_own(last + 1)

    ig_in[tp] = ig_part[tp]
    for step in range(1, n_tp):
        source = lax.rem(tp + step, n_tp)
        input_copy(source, source).wait_recv()
    for half in range(2):
        strip = ig_out.shape[0] // 2
        r = pl.ds(half * strip, strip)
        value = ig_in[0, r, :].astype(jnp.float32)
        for source in range(1, n_tp):
            value = value + ig_in[source, r, :].astype(jnp.float32)
        ig_out[r, :] = value.astype(ig_out.dtype)

    for p in range(parts):
        for kind in (DOWN, GATE, UP):
            reduce_final(3 * p + kind)

    def drain(i, carry):
        g, chip = i // nz, i % nz
        gather_copy(g, chip, SIBLING).wait_send()
        sibling_copy(g, chip).wait_send()

        @pl.when(jnp.logical_and(has_right, chip <= z))
        def _():
            gather_copy(g, chip, RIGHT).wait_send()

        @pl.when(jnp.logical_and(has_left, chip >= z))
        def _():
            gather_copy(g, chip, LEFT).wait_send()

        @pl.when(chip != z)
        def _():
            way = jnp.where(chip > z, RIGHT, LEFT)
            line_copy(g, way, chip).wait_send()

        return carry

    lax.fori_loop(0, 3 * parts * nz, drain, 0)
    for step in range(1, n_tp):
        input_copy(lax.rem(tp + step, n_tp), tp).wait_send()


PARTS = 2


def fused_shards(tokens, cotangent, gate_weight, up_weight, down_weight):
    n, n_tp = lax.axis_size("fs"), lax.axis_size("tp")
    nz = n // 2
    count, width = tokens.shape
    rows, hidden = gate_weight.shape
    height = hidden // PARTS
    pieces = 3 * PARTS
    share = width // n_tp
    bf16, f32 = jnp.bfloat16, jnp.float32
    dma = pltpu.SemaphoreType.DMA
    input_grad, gate_grad, up_grad, down_grad = pl.pallas_call(
        functools.partial(kernel, n, n_tp, PARTS),
        out_shape=(
            jax.ShapeDtypeStruct((count, share), bf16),
        ) + (jax.ShapeDtypeStruct((hidden, rows), f32),) * 3,
        in_specs=[pl.BlockSpec(memory_space=pl.ANY)] * 5,
        out_specs=(pl.BlockSpec(memory_space=pltpu.VMEM),) * 4,
        scratch_shapes=[
            pltpu.VMEM((2, count, width), bf16),
            pltpu.VMEM((pieces, n, height, rows), bf16),
            pltpu.VMEM((3, height, count), f32),
            pltpu.VMEM((pieces, height, count), bf16),
            pltpu.VMEM((pieces, height, rows), f32),
            pltpu.VMEM((pieces, nz, height, rows), bf16),
            pltpu.VMEM((pieces, nz, height, rows), bf16),
            pltpu.VMEM((pieces, nz, height, rows), bf16),
            pltpu.VMEM((pieces, 2, nz, height, rows), bf16),
            pltpu.VMEM((height, rows), f32),
            pltpu.VMEM((n_tp, count, share), bf16),
            pltpu.VMEM((n_tp, count, share), bf16),
            dma((pieces + 2,)),
            dma((pieces, 3, nz)),
            dma((pieces, n)),
            dma((pieces, nz)),
            dma((pieces, nz)),
            dma((pieces, nz)),
            dma((pieces, 2, nz)),
            dma((n_tp,)),
            dma((n_tp,)),
        ],
        compiler_params=pltpu.CompilerParams(
            collective_id=0, has_side_effects=True, vmem_limit_bytes=67043328
        ),
    )(tokens, cotangent, gate_weight.T, up_weight.T, down_weight.T)
    return input_grad, gate_grad.T, up_grad.T, down_grad.T


def shards(tokens, cotangent, gate_weight, up_weight, down_weight):
    n, n_tp = lax.axis_size("fs"), lax.axis_size("tp")
    rows = gate_weight.shape[0]
    share = tokens.shape[1] // n_tp
    if n % 2 == 0 and rows % 128 == 0 and share % rows == 0 and n <= 8 and (
        gate_weight.shape[1] % (16 * PARTS) == 0
    ):
        return fused_shards(tokens, cotangent, gate_weight, up_weight, down_weight)
    return plain_shards(tokens, cotangent, gate_weight, up_weight, down_weight)


def solution(mesh):
    in_specs = (P("fs", None), P("fs", None), P("fs", "tp"), P("fs", "tp"), P("fs", "tp"))
    out_specs = (P("fs", "tp"), P("fs", "tp"), P("fs", "tp"), P("fs", "tp"))
    return jax.shard_map(shards, mesh=mesh, in_specs=in_specs, out_specs=out_specs, check_vma=False)
```

profile of v0, /device:TPU:10, one launch (start us, length us, event | category | flops | bytes accessed | tf_op | source)
XLA Modules:
  0.0 144.3 jit_solution(360621216593345686)
XLA Ops:
  0.6 137.9 %shard_map.84 = (bf16[512,512]{1,0:T(8,128)(2,1)}, f32[704,256]{1,0:T(8,128)}, f32[704,256]{1,0:T(8,128)}, f32[704,256]{1,0:T(8,128)}) custom-call(bf16[512,2048]{1,0:T(8,128)(2,1)} %tok.1, bf16[512,2048]{1,0:T(8,128)(2,1)} %cot.1, bf16[704,256]{1,0:T(8,128)(2,1)} %bitcast.9, bf16[704,256]{1,0:T(8,128)(2,1)} %bitcast.10, bf16[704,256]{1,0:T(8,128)(2,1)} %bitcast.11), custom_call_target="tpu_custom_call" | custom-call | tf_op jit(solution)/shard_map/pallas_call | solution.py:471
  138.5 0.0 copy-start.1
  138.5 0.0 copy-start
  138.6 2.0 %copy.13 = bf16[512,512]{1,0:T(8,128)(2,1)} copy(bf16[512,512]{1,0:T(8,128)(2,1)} %get-tuple-element.16) | data formatting | bytes 1048576
  140.5 2.0 %copy.14 = f32[256,704]{0,1:T(8,128)} copy(f32[256,704]{0,1:T(8,128)} %bitcast.8) | data formatting | bytes 1441792
  142.5 0.0 copy-done.1
  142.5 0.9 copy.15
  143.4 0.0 copy-done
  143.4 0.9 copy.16
Async XLA Ops:
  138.5 4.0 %copy-start.1 = (f32[704,256]{1,0:T(8,128)S(1)}, f32[704,256]{1,0:T(8,128)}, u32[]{:S(2)}) copy-start(f32[704,256]{1,0:T(8,128)} %get-tuple-element.10) | copy-start | bytes 2162692
  138.5 4.9 %copy-start = (f32[704,256]{1,0:T(8,128)S(1)}, f32[704,256]{1,0:T(8,128)}, u32[]{:S(2)}) copy-start(f32[704,256]{1,0:T(8,128)} %get-tuple-element.11) | copy-start | bytes 2162692
where the time goes:
time: 144 us
  Pallas kernels  138 us (96%)
  local copies, waits for them, and re-layouts  5.71 us (4%)
    pallas_call x1, Pallas kernels, fused_shards(): pl.pallas_call(functools.partial(kernel, n, n_tp, PARTS), out_shape=(jax....  138 us
    unnamed x8, local copies, waits for them, and re-layouts  5.71 us

commit v1 on v0

v1 whole, which is shorter than its diff:
```python
import functools

import jax
import jax.numpy as jnp
from jax import lax
from jax.experimental import pallas as pl
from jax.experimental.pallas import tpu as pltpu
from jax.sharding import PartitionSpec as P


def row_product(left, right):
    return lax.dot_general(
        left, right, (((1,), (1,)), ((), ())), preferred_element_type=jnp.float32
    )


def token_product(left, right):
    return lax.dot_general(
        left, right, (((0,), (0,)), ((), ())), preferred_element_type=jnp.float32
    )


def owner_sum(received, groups):
    return received.reshape(groups, received.shape[0] // groups, received.shape[1]).sum(axis=0)


def plain_shards(tokens, cotangent, gate_weight, up_weight, down_weight):
    groups = lax.axis_size("fs")
    whole_gate, whole_up, whole_down = (
        lax.all_gather(gate_weight, "fs", axis=0, tiled=True),
        lax.all_gather(up_weight, "fs", axis=0, tiled=True),
        lax.all_gather(down_weight, "fs", axis=0, tiled=True),
    )
    gate = jnp.dot(tokens, whole_gate, preferred_element_type=jnp.float32)
    up = jnp.dot(tokens, whole_up, preferred_element_type=jnp.float32)
    hidden_grad = jnp.dot(cotangent, whole_down, preferred_element_type=jnp.float32)
    sig = jax.nn.sigmoid(gate)
    act = gate * sig
    hidden = (act * up).astype(jnp.bfloat16)
    gate_cot = (hidden_grad * up * sig * (1.0 + gate * (1.0 - sig))).astype(jnp.bfloat16)
    up_cot = (hidden_grad * act).astype(jnp.bfloat16)
    partial_value = row_product(gate_cot, whole_gate) + row_product(up_cot, whole_up)
    input_grad = lax.psum_scatter(
        partial_value.astype(jnp.bfloat16), "tp", scatter_dimension=1, tiled=True
    )
    gate_term = token_product(tokens, gate_cot)
    gate_grad = owner_sum(
        lax.all_to_all(
            gate_term.astype(jnp.bfloat16), "fs", split_axis=0, concat_axis=0, tiled=True
        ).astype(gate_term.dtype),
        groups,
    )
    up_term = token_product(tokens, up_cot)
    up_grad = owner_sum(
        lax.all_to_all(
            up_term.astype(jnp.bfloat16), "fs", split_axis=0, concat_axis=0, tiled=True
        ).astype(up_term.dtype),
        groups,
    )
    down_term = token_product(cotangent, hidden)
    down_grad = owner_sum(
        lax.all_to_all(
            down_term.astype(jnp.bfloat16), "fs", split_axis=0, concat_axis=0, tiled=True
        ).astype(down_term.dtype),
        groups,
    )
    return (input_grad, gate_grad, up_grad, down_grad)


MESH = pl.DeviceIdType.MESH
PARTS = 4
CHIPS = 4
LAG = 7
LAG_OUT = 1
OWN_IN, OWN_OUT = 2, 3
RELAY_IN, RELAY_OUT = 2, 1
GATE, UP, DOWN = 0, 1, 2
RIGHT, LEFT, SIBLING = 0, 1, 2


def kernel(
    n, n_tp, parts, tok, cot, gw, uw, dw, ig_out, gate_out, up_out, down_out,
    x, w_all, acc, cots, own_sum, sib_out, sib_in, line_out, line_in, ig_acc, ig_part, ig_in,
    local_sem, ag_send, ag_recv, sib_send, sib_recv, line_send, line_recv, ig_send, ig_recv,
):
    me, tp = lax.axis_index("fs"), lax.axis_index("tp")
    z, c = me // 2, me % 2
    nz = n // 2
    total = 3 * parts
    other = 2 * z + 1 - c
    rows = gw.shape[1]
    height = gw.shape[0] // parts
    own_columns = ig_out.shape[1]
    pieces = own_columns // rows
    mirrored = z >= nz // 2
    is_end = jnp.logical_or(z == 0, z == nz - 1)
    inward = jnp.where(mirrored, LEFT, RIGHT)
    outward = jnp.where(mirrored, RIGHT, LEFT)

    def chip_at(q):
        return jnp.where(mirrored, nz - 1 - q, q)

    def weight_load(t):
        piece = pl.ds((t // 3) * height, height)
        return pltpu.make_async_copy(
            (gw, uw, dw)[t % 3].at[piece, :], w_all.at[t, me], local_sem.at[t]
        )

    loads = [weight_load(t) for t in range(total)]
    loads += [
        pltpu.make_async_copy(tok, x.at[0], local_sem.at[total]),
        pltpu.make_async_copy(cot, x.at[1], local_sem.at[total + 1]),
    ]
    for load in loads:
        load.start()

    has_left, has_right = z > 0, z < nz - 1
    barrier = pltpu.get_barrier_semaphore()
    pl.semaphore_signal(barrier, inc=1, device_id={"fs": other}, device_id_type=MESH)
    for step in range(1, n_tp):
        pl.semaphore_signal(
            barrier, inc=1, device_id={"tp": lax.rem(tp + step, n_tp)}, device_id_type=MESH
        )

    @pl.when(has_right)
    def _():
        pl.semaphore_signal(barrier, inc=1, device_id={"fs": me + 2}, device_id_type=MESH)

    @pl.when(has_left)
    def _():
        pl.semaphore_signal(barrier, inc=1, device_id={"fs": me - 2}, device_id_type=MESH)

    pl.semaphore_wait(barrier, n_tp + has_left.astype(jnp.int32) + has_right.astype(jnp.int32))

    def line_device(way):
        return me + 2 - 4 * way

    def gather_copy(t, q, way):
        chip = chip_at(q)
        slot = 2 * chip + c
        device = other if way is SIBLING else line_device(way)
        return pltpu.make_async_remote_copy(
            src_ref=w_all.at[t, slot], dst_ref=w_all.at[t, slot],
            send_sem=ag_send.at[t, way, chip], recv_sem=ag_recv.at[t, slot],
            device_id={"fs": device}, device_id_type=MESH,
        )

    def gather_wait(t, q, core):
        slot = 2 * chip_at(q) + core
        pltpu.make_async_remote_copy(
            src_ref=w_all.at[t, slot], dst_ref=w_all.at[t, slot],
            send_sem=ag_send.at[t, SIBLING, 0], recv_sem=ag_recv.at[t, slot],
            device_id={"fs": other}, device_id_type=MESH,
        ).wait_recv()

    def columns_of(slot):
        return pl.ds(pl.multiple_of(slot * rows, rows), rows)

    def pair_product(t, kind, q, first):
        gather_wait(t, q, 1 - c)
        value = None
        for core in range(2):
            slot = 2 * chip_at(q) + core
            part = row_product(w_all[t, slot], x[kind // 2, :, columns_of(slot)])
            value = part if value is None else value + part
        if first:
            acc[kind] = value
        else:
            acc[kind] += value

    def by_rows(body):
        strip = 16

        def step(i, carry):
            body(pl.ds(pl.multiple_of(i * strip, strip), strip))
            return carry

        lax.fori_loop(0, height // strip, step, 0)

    def make_hidden(p):
        t = 3 * p + DOWN

        def strip(r):
            gate = acc[GATE, r, :]
            sig = jax.nn.sigmoid(gate)
            act = gate * sig
            up = acc[UP, r, :]
            cots[t, r, :] = (act * up).astype(jnp.bfloat16)
            acc[UP, r, :] = up * sig * (1.0 + gate * (1.0 - sig))
            acc[GATE, r, :] = act

        by_rows(strip)

    def make_cots(p):
        t = 3 * p

        def strip(r):
            hidden_grad = acc[DOWN, r, :]
            cots[t + GATE, r, :] = (hidden_grad * acc[UP, r, :]).astype(jnp.bfloat16)
            cots[t + UP, r, :] = (hidden_grad * acc[GATE, r, :]).astype(jnp.bfloat16)

        by_rows(strip)

    def side_of(g):
        return lax.rem(g, 3) // 2

    def term(g, slot):
        return jnp.dot(
            cots[g], x[side_of(g), :, columns_of(slot)], preferred_element_type=jnp.float32
        )

    def sibling_copy(g, chip):
        return pltpu.make_async_remote_copy(
            src_ref=sib_out.at[g, chip], dst_ref=sib_in.at[g, chip],
            send_sem=sib_send.at[g, chip], recv_sem=sib_recv.at[g, chip],
            device_id={"fs": other}, device_id_type=MESH,
        )

    def line_copy(g, way, chip):
        return pltpu.make_async_remote_copy(
            src_ref=line_out.at[g, chip], dst_ref=line_in.at[g, way, chip],
            send_sem=line_send.at[g, chip], recv_sem=line_recv.at[g, way, chip],
            device_id={"fs": line_device(way)}, device_id_type=MESH,
        )

    def sibling_terms(g, order):
        for q in order:
            chip = chip_at(q)
            sib_out[g, chip] = term(g, 2 * chip + 1 - c).astype(jnp.bfloat16)
            sibling_copy(g, chip).start()

    def pair_sum(g, chip):
        own = term(g, 2 * chip + c)
        sibling_copy(g, chip).wait_recv()
        return own + sib_in[g, chip].astype(jnp.float32)

    def send_sum(g, q, way, relay):
        chip = chip_at(q)
        value = pair_sum(g, chip)
        if relay:
            line_copy(g, way, chip).wait_recv()
            value = value + line_in[g, way, chip].astype(jnp.float32)
        line_out[g, chip] = value.astype(jnp.bfloat16)
        line_copy(g, way, chip).start()

    def input_copy(peer, source):
        return pltpu.make_async_remote_copy(
            src_ref=ig_part.at[peer], dst_ref=ig_in.at[source],
            send_sem=ig_send.at[peer], recv_sem=ig_recv.at[source],
            device_id={"tp": peer}, device_id_type=MESH,
        )

    def input_terms(p):
        def body(step, carry):
            peer = lax.rem(tp + 1 + step, n_tp)
            value = None
            for t in (3 * p + GATE, 3 * p + UP):
                block = jnp.concatenate(
                    [w_all[t, peer * pieces + i] for i in range(pieces)], axis=1
                )
                part = token_product(cots[t], block)
                value = part if value is None else value + part

            @pl.when(p == 0)
            def _():
                ig_acc[peer] = value

            @pl.when(jnp.logical_and(p > 0, p < parts - 1))
            def _():
                ig_acc[peer] += value

            @pl.when(p == parts - 1)
            def _():
                ig_part[peer] = (ig_acc[peer] + value).astype(jnp.bfloat16)

            @pl.when(jnp.logical_and(p == parts - 1, step < n_tp - 1))
            def _():
                input_copy(peer, tp).start()

            return carry

        lax.fori_loop(0, n_tp, body, 0)

    def end_gather(t, kind):
        gather_wait(t, 1, c)
        gather_copy(t, 1, SIBLING).start()
        pair_product(t, kind, 0, True)
        gather_wait(t, 2, c)
        gather_copy(t, 2, SIBLING).start()
        pair_product(t, kind, 1, False)
        gather_wait(t, 3, c)
        gather_copy(t, 3, SIBLING).start()
        pair_product(t, kind, 2, False)
        pair_product(t, kind, 3, False)

    def end_reduce(low, high):
        def terms(g, carry):
            sibling_terms(g, (3, 2, 1, 0))
            return carry

        def far(g, carry):
            for q in (3, 2):
                send_sum(g, q, inward, False)
            return carry

        def near(g, carry):
            send_sum(g, 1, inward, False)
            own_sum[g] = pair_sum(g, z)
            return carry

        for body in (terms, far, near):
            lax.fori_loop(low, high, body, 0)

    def end_part(p, carry):
        end_gather(3 * p + GATE, GATE)
        end_gather(3 * p + UP, UP)
        make_hidden(p)
        end_reduce(3 * p + DOWN, 3 * p + DOWN + 1)

        @pl.when(p > 0)
        def _():
            input_terms(p - 1)

        end_gather(3 * p + DOWN, DOWN)
        make_cots(p)

        @pl.when(p == parts - 1)
        def _():
            input_terms(p)

        end_reduce(3 * p + GATE, 3 * p + DOWN)
        return carry

    def relay_in(t):
        @pl.when(t < total)
        def _():
            gather_wait(t, 0, c)
            gather_copy(t, 0, inward).start()
            gather_copy(t, 0, SIBLING).start()

        @pl.when(t + OWN_IN < total)
        def _():
            gather_copy(t + OWN_IN, 1, inward).start()

    def relay_near(t):
        @pl.when(t < total)
        def _():
            gather_wait(t, 2, c)
            gather_copy(t, 2, outward).start()
            gather_copy(t, 2, SIBLING).start()

    def relay_far(t):
        @pl.when(t < total)
        def _():
            gather_wait(t, 3, c)
            gather_copy(t, 3, outward).start()
            gather_copy(t, 3, SIBLING).start()

        @pl.when(t + OWN_OUT < total)
        def _():
            gather_copy(t + OWN_OUT, 1, outward).start()

    def middle_gather(t, kind):
        relay_in(t + RELAY_IN)
        pair_product(t, kind, 1, True)
        relay_near(t + RELAY_OUT)
        pair_product(t, kind, 0, False)
        relay_far(t + RELAY_OUT)
        pair_product(t, kind, 2, False)
        pair_product(t, kind, 3, False)

    def in_turn(i):
        return 3 * (i // 3) + lax.rem(i + 2, 3)

    def middle_reduce(r):
        @pl.when(jnp.logical_and(r >= -1, r < total - 1))
        def _():
            sibling_terms(in_turn(r + 1), (3, 2, 0, 1))

        @pl.when(jnp.logical_and(r >= 0, r < total))
        def _():
            g = in_turn(r)
            send_sum(g, 3, inward, True)
            send_sum(g, 2, inward, True)
            own_sum[g] = pair_sum(g, z)

        @pl.when(r >= LAG_OUT)
        def _():
            send_sum(in_turn(r - LAG_OUT), 0, outward, True)

    def middle_part(p, carry):
        for kind in (GATE, UP, DOWN):
            t = 3 * p + kind
            middle_gather(t, kind)
            if kind == UP:
                make_hidden(p)
            if kind == DOWN:
                make_cots(p)
            middle_reduce(t - LAG)
        input_terms(p)
        return carry

    def middle_rest(r, carry):
        middle_reduce(r)
        return carry

    for t in range(total):
        loads[t].wait()
        gather_copy(t, jnp.where(is_end, 0, 1), SIBLING).start()

        @pl.when(is_end)
        def _():
            gather_copy(t, 0, inward).start()

        if t < OWN_OUT:
            @pl.when(jnp.logical_not(is_end))
            def _():
                gather_copy(t, 1, outward).start()

        if t < OWN_IN:
            @pl.when(jnp.logical_not(is_end))
            def _():
                gather_copy(t, 1, inward).start()

    loads[total].wait()
    loads[total + 1].wait()

    @pl.when(is_end)
    def _():
        lax.fori_loop(0, parts, end_part, 0)

    @pl.when(jnp.logical_not(is_end))
    def _():
        for t in range(RELAY_IN):
            relay_in(t)
        for t in range(RELAY_OUT):
            relay_near(t)
            relay_far(t)
        lax.fori_loop(0, parts, middle_part, 0)
        lax.fori_loop(total - LAG, total + LAG_OUT, middle_rest, 0)

    ig_in[tp] = ig_part[tp]
    for step in range(1, n_tp):
        source = lax.rem(tp + step, n_tp)
        input_copy(source, source).wait_recv()
    for half in range(2):
        strip = ig_out.shape[0] // 2
        r = pl.ds(half * strip, strip)
        value = ig_in[0, r, :].astype(jnp.float32)
        for source in range(1, n_tp):
            value = value + ig_in[source, r, :].astype(jnp.float32)
        ig_out[r, :] = value.astype(ig_out.dtype)

    for p in range(parts):
        for kind in (DOWN, GATE, UP):
            g = 3 * p + kind
            piece = pl.ds(p * height, height)
            out = (gate_out, up_out, down_out)[kind]
            line_copy(g, outward, z).wait_recv()
            value = own_sum[g] + line_in[g, outward, z].astype(jnp.float32)
            out[piece, :] = value

            @pl.when(jnp.logical_not(is_end))
            def _():
                line_copy(g, inward, z).wait_recv()
                out[piece, :] += line_in[g, inward, z].astype(jnp.float32)

    def drain(g, carry):
        for chip in range(nz):
            gather_copy(g, chip, SIBLING).wait_send()
            sibling_copy(g, chip).wait_send()

            @pl.when(chip != z)
            def _():
                way = jnp.where(chip > z, RIGHT, LEFT)
                line_copy(g, way, chip).wait_send()

            @pl.when(jnp.logical_and(has_right, chip <= z))
            def _():
                absolute_copy(g, chip, RIGHT).wait_send()

            @pl.when(jnp.logical_and(has_left, chip >= z))
            def _():
                absolute_copy(g, chip, LEFT).wait_send()

        return carry

    def absolute_copy(t, chip, way):
        slot = 2 * chip + c
        return pltpu.make_async_remote_copy(
            src_ref=w_all.at[t, slot], dst_ref=w_all.at[t, slot],
            send_sem=ag_send.at[t, way, chip], recv_sem=ag_recv.at[t, slot],
            device_id={"fs": line_device(way)}, device_id_type=MESH,
        )

    lax.fori_loop(0, total, drain, 0)
    for step in range(1, n_tp):
        input_copy(lax.rem(tp + step, n_tp), tp).wait_send()


def fused_shards(tokens, cotangent, gate_weight, up_weight, down_weight):
    n, n_tp = lax.axis_size("fs"), lax.axis_size("tp")
    nz = n // 2
    count, width = tokens.shape
    rows, hidden = gate_weight.shape
    height = hidden // PARTS
    pieces = 3 * PARTS
    share = width // n_tp
    bf16, f32 = jnp.bfloat16, jnp.float32
    dma = pltpu.SemaphoreType.DMA
    input_grad, gate_grad, up_grad, down_grad = pl.pallas_call(
        functools.partial(kernel, n, n_tp, PARTS),
        out_shape=(
            jax.ShapeDtypeStruct((count, share), bf16),
        ) + (jax.ShapeDtypeStruct((hidden, rows), f32),) * 3,
        in_specs=[pl.BlockSpec(memory_space=pl.ANY)] * 5,
        out_specs=(pl.BlockSpec(memory_space=pltpu.VMEM),) * 4,
        scratch_shapes=[
            pltpu.VMEM((2, count, width), bf16),
            pltpu.VMEM((pieces, n, height, rows), bf16),
            pltpu.VMEM((3, height, count), f32),
            pltpu.VMEM((pieces, height, count), bf16),
            pltpu.VMEM((pieces, height, rows), f32),
            pltpu.VMEM((pieces, nz, height, rows), bf16),
            pltpu.VMEM((pieces, nz, height, rows), bf16),
            pltpu.VMEM((pieces, nz, height, rows), bf16),
            pltpu.VMEM((pieces, 2, nz, height, rows), bf16),
            pltpu.VMEM((n_tp, count, share), f32),
            pltpu.VMEM((n_tp, count, share), bf16),
            pltpu.VMEM((n_tp, count, share), bf16),
            dma((pieces + 2,)),
            dma((pieces, 3, nz)),
            dma((pieces, n)),
            dma((pieces, nz)),
            dma((pieces, nz)),
            dma((pieces, nz)),
            dma((pieces, 2, nz)),
            dma((n_tp,)),
            dma((n_tp,)),
        ],
        compiler_params=pltpu.CompilerParams(
            collective_id=0, has_side_effects=True, vmem_limit_bytes=67043328
        ),
    )(tokens, cotangent, gate_weight.T, up_weight.T, down_weight.T)
    return input_grad, gate_grad.T, up_grad.T, down_grad.T


def shards(tokens, cotangent, gate_weight, up_weight, down_weight):
    n, n_tp = lax.axis_size("fs"), lax.axis_size("tp")
    rows = gate_weight.shape[0]
    share = tokens.shape[1] // n_tp
    if n == 2 * CHIPS and rows % 128 == 0 and share % rows == 0 and (
        gate_weight.shape[1] % (16 * PARTS) == 0
    ):
        return fused_shards(tokens, cotangent, gate_weight, up_weight, down_weight)
    return plain_shards(tokens, cotangent, gate_weight, up_weight, down_weight)


def solution(mesh):
    in_specs = (P("fs", None), P("fs", None), P("fs", "tp"), P("fs", "tp"), P("fs", "tp"))
    out_specs = (P("fs", "tp"), P("fs", "tp"), P("fs", "tp"), P("fs", "tp"))
    return jax.shard_map(shards, mesh=mesh, in_specs=in_specs, out_specs=out_specs, check_vma=False)
```

time: 144 us -> 125 us (0.87)
  the two profiles are of different devices: /device:TPU:10 before, /device:TPU:0 now
where the time goes in v1:
time: 125 us
  Pallas kernels  118 us (94%)
  local copies, waits for them, and re-layouts  5.71 us (5%)
    pallas_call x1, Pallas kernels, fused_shards(): pl.pallas_call(functools.partial(kernel, n, n_tp, PARTS), out_shape=(jax....  118 us
    unnamed x8, local copies, waits for them, and re-layouts  5.71 us

profile of v1, /device:TPU:0, one launch (start us, length us, event | category | flops | bytes accessed | tf_op | source)
XLA Modules:
  0.0 124.6 jit_solution(5315728360108986254)
XLA Ops:
  0.6 118.2 %shard_map.84 = (bf16[512,512]{1,0:T(8,128)(2,1)}, f32[704,256]{1,0:T(8,128)}, f32[704,256]{1,0:T(8,128)}, f32[704,256]{1,0:T(8,128)}) custom-call(bf16[512,2048]{1,0:T(8,128)(2,1)} %tok.1, bf16[512,2048]{1,0:T(8,128)(2,1)} %cot.1, bf16[704,256]{1,0:T(8,128)(2,1)} %bitcast.9, bf16[704,256]{1,0:T(8,128)(2,1)} %bitcast.10, bf16[704,256]{1,0:T(8,128)(2,1)} %bitcast.11), custom_call_target="tpu_custom_call" | custom-call | tf_op jit(solution)/shard_map/pallas_call | solution.py:511
  118.8 0.0 copy-start.1
  118.8 0.0 copy-start
  118.8 2.0 %copy.13 = bf16[512,512]{1,0:T(8,128)(2,1)} copy(bf16[512,512]{1,0:T(8,128)(2,1)} %get-tuple-element.16) | data formatting | bytes 1048576
  120.8 2.0 %copy.14 = f32[256,704]{0,1:T(8,128)} copy(f32[256,704]{0,1:T(8,128)} %bitcast.8) | data formatting | bytes 1441792
  122.8 0.0 copy-done.1
  122.8 0.9 copy.15
  123.7 0.0 copy-done
  123.7 0.9 copy.16
Async XLA Ops:
  118.8 4.0 %copy-start.1 = (f32[704,256]{1,0:T(8,128)S(1)}, f32[704,256]{1,0:T(8,128)}, u32[]{:S(2)}) copy-start(f32[704,256]{1,0:T(8,128)} %get-tuple-element.10) | copy-start | bytes 2162692
  118.8 4.9 %copy-start = (f32[704,256]{1,0:T(8,128)S(1)}, f32[704,256]{1,0:T(8,128)}, u32[]{:S(2)}) copy-start(f32[704,256]{1,0:T(8,128)} %get-tuple-element.11) | copy-start | bytes 2162692

commit v2 on v1

--- a/solution.py
+++ b/solution.py
@@ -71,7 +71,11 @@
 PARTS = 4
 CHIPS = 4
 LAG = 7
+VMEM_BYTES = 56 * 1024 * 1024
+DELIVER_BYTES = 1024 * 1024
 LAG_OUT = 1
+LAG_FINAL = 4
+INPUT_TURN = 3
 OWN_IN, OWN_OUT = 2, 3
 RELAY_IN, RELAY_OUT = 2, 1
 GATE, UP, DOWN = 0, 1, 2
@@ -79,8 +83,8 @@
 
 
 def kernel(
-    n, n_tp, parts, tok, cot, gw, uw, dw, ig_out, gate_out, up_out, down_out,
-    x, w_all, acc, cots, own_sum, sib_out, sib_in, line_out, line_in, ig_acc, ig_part, ig_in,
+    n, n_tp, parts, tok, cot, gw, uw, dw, ig_out, own_sum,
+    x, w_all, acc, cots, sib_out, sib_in, line_out, line_in, ig_acc, ig_part, ig_in, ig_mid,
     local_sem, ag_send, ag_recv, sib_send, sib_recv, line_send, line_recv, ig_send, ig_recv,
 ):
     me, tp = lax.axis_index("fs"), lax.axis_index("tp")
@@ -243,16 +247,43 @@
         line_out[g, chip] = value.astype(jnp.bfloat16)
         line_copy(g, way, chip).start()
 
-    def input_copy(peer, source):
+    side_peer = tp + 1 - 2 * lax.rem(tp, 2)
+    far_peer = lax.rem(tp + 2, n_tp)
+    corner = lax.rem(side_peer + 2, n_tp)
+    half = ig_out.shape[0] // 2
+
+    def half_rows(s):
+        return pl.ds(s * half, half)
+
+    def input_copy(k, source):
+        s = k % 2
+        peers = (side_peer, far_peer) if k < 4 else (far_peer, side_peer)
         return pltpu.make_async_remote_copy(
-            src_ref=ig_part.at[peer], dst_ref=ig_in.at[source],
-            send_sem=ig_send.at[peer], recv_sem=ig_recv.at[source],
-            device_id={"tp": peer}, device_id_type=MESH,
-        )
+            src_ref=source, dst_ref=ig_in.at[k], send_sem=ig_send.at[k], recv_sem=ig_recv.at[k],
+            device_id={"tp": peers[s]}, device_id_type=MESH,
+        )
+
+    def corner_copy(s):
+        return input_copy(s, ig_part.at[corner, half_rows(s), :])
+
+    def direct_copy(s):
+        return input_copy(2 + s, ig_part.at[(side_peer, far_peer)[s], half_rows(s), :])
+
+    def relay_copy(s):
+        return input_copy(4 + s, ig_mid.at[s])
+
+    def input_relay():
+        for s in range(2):
+            corner_copy(s).wait_recv()
+            own = ig_part[(far_peer, side_peer)[s], half_rows(s), :].astype(jnp.float32)
+            ig_mid[s] = (own + ig_in[s].astype(jnp.float32)).astype(jnp.bfloat16)
+            relay_copy(s).start()
 
     def input_terms(p):
         def body(step, carry):
-            peer = lax.rem(tp + 1 + step, n_tp)
+            peer = jnp.where(
+                step == 0, corner, jnp.where(step == 1, side_peer, jnp.where(step == 2, far_peer, tp))
+            )
             value = None
             for t in (3 * p + GATE, 3 * p + UP):
                 block = jnp.concatenate(
@@ -273,9 +304,18 @@
             def _():
                 ig_part[peer] = (ig_acc[peer] + value).astype(jnp.bfloat16)
 
-            @pl.when(jnp.logical_and(p == parts - 1, step < n_tp - 1))
-            def _():
-                input_copy(peer, tp).start()
+            @pl.when(jnp.logical_and(p == parts - 1, step == 0))
+            def _():
+                corner_copy(0).start()
+                corner_copy(1).start()
+
+            @pl.when(jnp.logical_and(p == parts - 1, step == 1))
+            def _():
+                direct_copy(0).start()
+
+            @pl.when(jnp.logical_and(p == parts - 1, step == 2))
+            def _():
+                direct_copy(1).start()
 
             return carry
 
@@ -372,6 +412,21 @@
     def in_turn(i):
         return 3 * (i // 3) + lax.rem(i + 2, 3)
 
+    def final(r, carry):
+        g = in_turn(r)
+        line_copy(g, outward, z).wait_recv()
+        own_sum[g] += line_in[g, outward, z].astype(jnp.float32)
+        return carry
+
+    def middle_final(r, carry):
+        g = in_turn(r)
+        for way in (inward, outward):
+            line_copy(g, way, z).wait_recv()
+        own_sum[g] += (
+            line_in[g, inward, z].astype(jnp.float32) + line_in[g, outward, z].astype(jnp.float32)
+        )
+        return carry
+
     def middle_reduce(r):
         @pl.when(jnp.logical_and(r >= -1, r < total - 1))
         def _():
@@ -387,6 +442,10 @@
         @pl.when(r >= LAG_OUT)
         def _():
             send_sum(in_turn(r - LAG_OUT), 0, outward, True)
+
+        @pl.when(r >= LAG_FINAL)
+        def _():
+            middle_final(r - LAG_FINAL, 0)
 
     def middle_part(p, carry):
         for kind in (GATE, UP, DOWN):
@@ -402,6 +461,11 @@
 
     def middle_rest(r, carry):
         middle_reduce(r)
+
+        @pl.when(r == total - INPUT_TURN)
+        def _():
+            input_relay()
+
         return carry
 
     for t in range(total):
@@ -428,6 +492,8 @@
     @pl.when(is_end)
     def _():
         lax.fori_loop(0, parts, end_part, 0)
+        input_relay()
+        lax.fori_loop(0, total, final, 0)
 
     @pl.when(jnp.logical_not(is_end))
     def _():
@@ -438,32 +504,15 @@
             relay_far(t)
         lax.fori_loop(0, parts, middle_part, 0)
         lax.fori_loop(total - LAG, total + LAG_OUT, middle_rest, 0)
-
-    ig_in[tp] = ig_part[tp]
-    for step in range(1, n_tp):
-        source = lax.rem(tp + step, n_tp)
-        input_copy(source, source).wait_recv()
-    for half in range(2):
-        strip = ig_out.shape[0] // 2
-        r = pl.ds(half * strip, strip)
-        value = ig_in[0, r, :].astype(jnp.float32)
-        for source in range(1, n_tp):
-            value = value + ig_in[source, r, :].astype(jnp.float32)
-        ig_out[r, :] = value.astype(ig_out.dtype)
-
-    for p in range(parts):
-        for kind in (DOWN, GATE, UP):
-            g = 3 * p + kind
-            piece = pl.ds(p * height, height)
-            out = (gate_out, up_out, down_out)[kind]
-            line_copy(g, outward, z).wait_recv()
-            value = own_sum[g] + line_in[g, outward, z].astype(jnp.float32)
-            out[piece, :] = value
-
-            @pl.when(jnp.logical_not(is_end))
-            def _():
-                line_copy(g, inward, z).wait_recv()
-                out[piece, :] += line_in[g, inward, z].astype(jnp.float32)
+        lax.fori_loop(total + LAG_OUT - LAG_FINAL, total, middle_final, 0)
+
+    for s in range(2):
+        direct_copy(s).wait_recv()
+        relay_copy(s).wait_recv()
+        value = ig_part[tp, half_rows(s), :].astype(jnp.float32)
+        for k in (2 + s, 4 + s):
+            value = value + ig_in[k].astype(jnp.float32)
+        ig_out[half_rows(s), :] = value.astype(ig_out.dtype)
 
     def drain(g, carry):
         for chip in range(nz):
@@ -494,8 +543,9 @@
         )
 
     lax.fori_loop(0, total, drain, 0)
-    for step in range(1, n_tp):
-        input_copy(lax.rem(tp + step, n_tp), tp).wait_send()
+    for s in range(2):
+        for copy in (corner_copy, direct_copy, relay_copy):
+            copy(s).wait_send()
 
 
 def fused_shards(tokens, cotangent, gate_weight, up_weight, down_weight):
@@ -508,26 +558,24 @@
     share = width // n_tp
     bf16, f32 = jnp.bfloat16, jnp.float32
     dma = pltpu.SemaphoreType.DMA
-    input_grad, gate_grad, up_grad, down_grad = pl.pallas_call(
+    input_grad, sums = pl.pallas_call(
         functools.partial(kernel, n, n_tp, PARTS),
-        out_shape=(
-            jax.ShapeDtypeStruct((count, share), bf16),
-        ) + (jax.ShapeDtypeStruct((hidden, rows), f32),) * 3,
+        out_shape=(pltpu.VMEM((count, share), bf16), pltpu.VMEM((pieces, height, rows), f32)),
         in_specs=[pl.BlockSpec(memory_space=pl.ANY)] * 5,
-        out_specs=(pl.BlockSpec(memory_space=pltpu.VMEM),) * 4,
+        out_specs=(pl.BlockSpec(memory_space=pltpu.VMEM),) * 2,
         scratch_shapes=[
             pltpu.VMEM((2, count, width), bf16),
             pltpu.VMEM((pieces, n, height, rows), bf16),
             pltpu.VMEM((3, height, count), f32),
             pltpu.VMEM((pieces, height, count), bf16),
-            pltpu.VMEM((pieces, height, rows), f32),
             pltpu.VMEM((pieces, nz, height, rows), bf16),
             pltpu.VMEM((pieces, nz, height, rows), bf16),
             pltpu.VMEM((pieces, nz, height, rows), bf16),
             pltpu.VMEM((pieces, 2, nz, height, rows), bf16),
             pltpu.VMEM((n_tp, count, share), f32),
             pltpu.VMEM((n_tp, count, share), bf16),
-            pltpu.VMEM((n_tp, count, share), bf16),
+            pltpu.VMEM((6, count // 2, share), bf16),
+            pltpu.VMEM((2, count // 2, share), bf16),
             dma((pieces + 2,)),
             dma((pieces, 3, nz)),
             dma((pieces, n)),
@@ -535,21 +583,44 @@
             dma((pieces, nz)),
             dma((pieces, nz)),
             dma((pieces, 2, nz)),
-            dma((n_tp,)),
-            dma((n_tp,)),
+            dma((6,)),
+            dma((6,)),
         ],
         compiler_params=pltpu.CompilerParams(
-            collective_id=0, has_side_effects=True, vmem_limit_bytes=67043328
+            collective_id=0, has_side_effects=True, vmem_limit_bytes=VMEM_BYTES
         ),
     )(tokens, cotangent, gate_weight.T, up_weight.T, down_weight.T)
+    input_grad, gate_grad, up_grad, down_grad = pl.pallas_call(
+        functools.partial(deliver, PARTS),
+        out_shape=(
+            jax.ShapeDtypeStruct((count, share), bf16),
+        ) + (jax.ShapeDtypeStruct((hidden, rows), f32),) * 3,
+        in_specs=[pl.BlockSpec(memory_space=pltpu.VMEM)] * 2,
+        out_specs=(pl.BlockSpec(memory_space=pl.ANY),) * 4,
+        scratch_shapes=[dma((pieces + 1,))],
+        compiler_params=pltpu.CompilerParams(vmem_limit_bytes=DELIVER_BYTES),
+    )(*(pltpu.with_memory_space_constraint(v, pltpu.VMEM) for v in (input_grad, sums)))
     return input_grad, gate_grad.T, up_grad.T, down_grad.T
+
+
+def deliver(parts, ig, sums, ig_out, gate_out, up_out, down_out, sem):
+    height = sums.shape[1]
+    copies = [pltpu.make_async_copy(ig, ig_out, sem.at[3 * parts])]
+    for g in range(3 * parts):
+        out = (gate_out, up_out, down_out)[g % 3]
+        piece = pl.ds((g // 3) * height, height)
+        copies.append(pltpu.make_async_copy(sums.at[g], out.at[piece, :], sem.at[g]))
+    for copy in copies:
+        copy.start()
+    for copy in copies:
+        copy.wait()
 
 
 def shards(tokens, cotangent, gate_weight, up_weight, down_weight):
     n, n_tp = lax.axis_size("fs"), lax.axis_size("tp")
     rows = gate_weight.shape[0]
     share = tokens.shape[1] // n_tp
-    if n == 2 * CHIPS and rows % 128 == 0 and share % rows == 0 and (
+    if n == 2 * CHIPS and n_tp == 4 and rows % 128 == 0 and share % rows == 0 and (
         gate_weight.shape[1] % (16 * PARTS) == 0
     ):
         return fused_shards(tokens, cotangent, gate_weight, up_weight, down_weight)

time: 125 us -> 115 us (0.920)
  local copies, waits for them, and re-layouts: 5.71 us -> 0 us
  Pallas kernels: 118 us -> 114 us
    unnamed x8 -> x0, local copies, waits for them, and re-layouts: 5.71 us -> none
    pallas_call x1 -> x2, Pallas kernels: 118 us -> 114 us  [the longest x1 112 us: fused_shards(): pl.pallas_call(functools.partial(kernel, n, n_tp, PARTS), out_shape=(pltp...]
where the time goes in v2:
time: 115 us
  Pallas kernels  114 us (99%)
    pallas_call x1, Pallas kernels, fused_shards(): pl.pallas_call(functools.partial(kernel, n, n_tp, PARTS), out_shape=(pltp...  112 us

profile of v2, /device:TPU:0, one launch (start us, length us, event | category | flops | bytes accessed | tf_op | source)
XLA Modules:
  0.0 114.6 jit_solution(8361305499782077974)
XLA Ops:
  0.6 112.2 %shard_map.84 = (bf16[512,512]{1,0:T(8,128)(2,1)S(1)}, f32[12,176,256]{2,1,0:T(8,128)S(1)}) custom-call(bf16[512,2048]{1,0:T(8,128)(2,1)} %tok.1, bf16[512,2048]{1,0:T(8,128)(2,1)} %cot.1, bf16[704,256]{1,0:T(8,128)(2,1)} %bitcast.6, bf16[704,256]{1,0:T(8,128)(2,1)} %bitcast.7, bf16[704,256]{1,0:T(8,128)(2,1)} %bitcast.8), custom_call_target="tpu_custom_call" | custom-call | tf_op jit(solution)/shard_map/pallas_call | solution.py:561
  112.8 1.6 %shard_map.85 = (bf16[512,512]{1,0:T(8,128)(2,1)}, f32[704,256]{1,0:T(8,128)}, f32[704,256]{1,0:T(8,128)}, f32[704,256]{1,0:T(8,128)}) custom-call(bf16[512,512]{1,0:T(8,128)(2,1)S(1)} %get-tuple-element.10.ig, f32[12,176,256]{2,1,0:T(8,128)S(1)} %get-tuple-element.11.sums), custom_call_target="tpu_custom_call" | custom-call | tf_op jit(solution)/shard_map/pallas_call | solution.py:593

commit v3 on v2

--- a/solution.py
+++ b/solution.py
@@ -71,11 +71,10 @@
 PARTS = 4
 CHIPS = 4
 LAG = 7
-VMEM_BYTES = 56 * 1024 * 1024
+VMEM_BYTES = 60 * 1024 * 1024
 DELIVER_BYTES = 1024 * 1024
-LAG_OUT = 1
-LAG_FINAL = 4
-INPUT_TURN = 3
+LAG_OUT, LAG_NEAR, LAG_FINAL = 2, 1, 5
+INPUT_TURN = 5
 OWN_IN, OWN_OUT = 2, 3
 RELAY_IN, RELAY_OUT = 2, 1
 GATE, UP, DOWN = 0, 1, 2
@@ -84,7 +83,7 @@
 
 def kernel(
     n, n_tp, parts, tok, cot, gw, uw, dw, ig_out, own_sum,
-    x, w_all, acc, cots, sib_out, sib_in, line_out, line_in, ig_acc, ig_part, ig_in, ig_mid,
+    x, w_all, acc, cots, cots_turned, own_term, sib_out, sib_in, line_out, line_in, ig_acc, ig_part, ig_in, ig_mid,
     local_sem, ag_send, ag_recv, sib_send, sib_recv, line_send, line_recv, ig_send, ig_recv,
 ):
     me, tp = lax.axis_index("fs"), lax.axis_index("tp")
@@ -228,15 +227,20 @@
         )
 
     def sibling_terms(g, order):
+        values = [term(g, 2 * chip_at(q) + 1 - c).astype(jnp.bfloat16) for q in order]
+        for q, value in zip(order, values):
+            sib_out[g, chip_at(q)] = value
         for q in order:
-            chip = chip_at(q)
-            sib_out[g, chip] = term(g, 2 * chip + 1 - c).astype(jnp.bfloat16)
-            sibling_copy(g, chip).start()
+            sibling_copy(g, chip_at(q)).start()
+
+    def own_terms(g, order):
+        values = [term(g, 2 * chip_at(q) + c) for q in order]
+        for q, value in zip(order, values):
+            own_term[g, chip_at(q)] = value
 
     def pair_sum(g, chip):
-        own = term(g, 2 * chip + c)
         sibling_copy(g, chip).wait_recv()
-        return own + sib_in[g, chip].astype(jnp.float32)
+        return own_term[g, chip] + sib_in[g, chip].astype(jnp.float32)
 
     def send_sum(g, q, way, relay):
         chip = chip_at(q)
@@ -279,41 +283,49 @@
             ig_mid[s] = (own + ig_in[s].astype(jnp.float32)).astype(jnp.bfloat16)
             relay_copy(s).start()
 
-    def input_terms(p):
+    def turn_cots(p):
+        for kind in (GATE, UP):
+            cots_turned[2 * p + kind] = cots[3 * p + kind].T
+
+    def input_value(peer, some_parts):
+        value = None
+        for p in some_parts:
+            for kind in (GATE, UP):
+                block = jnp.concatenate(
+                    [w_all[3 * p + kind, peer * pieces + i] for i in range(pieces)], axis=1
+                )
+                part = jnp.dot(
+                    cots_turned[2 * p + kind], block, preferred_element_type=jnp.float32
+                )
+                value = part if value is None else value + part
+        return value
+
+    def input_base(turn):
+        def body(peer, carry):
+            ig_acc[peer] = input_value(peer, range(parts - 1))
+            return carry
+
+        share = n_tp // 2
+        lax.fori_loop(turn * share, (turn + 1) * share, body, 0)
+
+    def input_last():
         def body(step, carry):
             peer = jnp.where(
                 step == 0, corner, jnp.where(step == 1, side_peer, jnp.where(step == 2, far_peer, tp))
             )
-            value = None
-            for t in (3 * p + GATE, 3 * p + UP):
-                block = jnp.concatenate(
-                    [w_all[t, peer * pieces + i] for i in range(pieces)], axis=1
-                )
-                part = token_product(cots[t], block)
-                value = part if value is None else value + part
-
-            @pl.when(p == 0)
-            def _():
-                ig_acc[peer] = value
-
-            @pl.when(jnp.logical_and(p > 0, p < parts - 1))
-            def _():
-                ig_acc[peer] += value
-
-            @pl.when(p == parts - 1)
-            def _():
-                ig_part[peer] = (ig_acc[peer] + value).astype(jnp.bfloat16)
-
-            @pl.when(jnp.logical_and(p == parts - 1, step == 0))
+            value = ig_acc[peer] + input_value(peer, (parts - 1,))
+            ig_part[peer] = value.astype(jnp.bfloat16)
+
+            @pl.when(step == 0)
             def _():
                 corner_copy(0).start()
                 corner_copy(1).start()
 
-            @pl.when(jnp.logical_and(p == parts - 1, step == 1))
+            @pl.when(step == 1)
             def _():
                 direct_copy(0).start()
 
-            @pl.when(jnp.logical_and(p == parts - 1, step == 2))
+            @pl.when(step == 2)
             def _():
                 direct_copy(1).start()
 
@@ -333,42 +345,68 @@
         pair_product(t, kind, 2, False)
         pair_product(t, kind, 3, False)
 
-    def end_reduce(low, high):
+    def end_terms(low, high):
         def terms(g, carry):
             sibling_terms(g, (3, 2, 1, 0))
             return carry
 
-        def far(g, carry):
-            for q in (3, 2):
+        def own(g, carry):
+            own_terms(g, (3, 2, 1, 0))
+            return carry
+
+        lax.fori_loop(low, high, terms, 0)
+        lax.fori_loop(low, high, own, 0)
+
+    def end_far(low, high):
+        for q in (3, 2):
+            def far(g, carry):
                 send_sum(g, q, inward, False)
-            return carry
-
+                return carry
+
+            lax.fori_loop(low, high, far, 0)
+
+    def end_near(low, high):
         def near(g, carry):
             send_sum(g, 1, inward, False)
             own_sum[g] = pair_sum(g, z)
             return carry
 
-        for body in (terms, far, near):
-            lax.fori_loop(low, high, body, 0)
+        lax.fori_loop(low, high, near, 0)
 
     def end_part(p, carry):
-        end_gather(3 * p + GATE, GATE)
-        end_gather(3 * p + UP, UP)
+        first = 3 * p
+        down = first + DOWN
+        is_last = (p == parts - 1).astype(jnp.int32)
+
+        def gate_or_up(kind, carry):
+            @pl.when(p == parts - 1)
+            def _():
+                input_base(kind)
+
+            end_gather(first + kind, kind)
+            return carry
+
+        lax.fori_loop(GATE, DOWN, gate_or_up, 0)
         make_hidden(p)
-        end_reduce(3 * p + DOWN, 3 * p + DOWN + 1)
-
-        @pl.when(p > 0)
-        def _():
-            input_terms(p - 1)
-
-        end_gather(3 * p + DOWN, DOWN)
+        end_terms(down, down + 1)
+        end_far(down, down + 1)
+        end_near(down + is_last, down + 1)
+
+        end_gather(down, DOWN)
         make_cots(p)
 
         @pl.when(p == parts - 1)
         def _():
-            input_terms(p)
-
-        end_reduce(3 * p + GATE, 3 * p + DOWN)
+            turn_cots(p)
+            input_last()
+
+        end_terms(first, down)
+        end_far(first, down)
+        end_near(first, down + is_last)
+
+        @pl.when(p < parts - 1)
+        def _():
+            turn_cots(p)
         return carry
 
     def relay_in(t):
@@ -430,18 +468,23 @@
     def middle_reduce(r):
         @pl.when(jnp.logical_and(r >= -1, r < total - 1))
         def _():
-            sibling_terms(in_turn(r + 1), (3, 2, 0, 1))
+            g = in_turn(r + 1)
+            sibling_terms(g, (3, 2, 0, 1))
+            own_terms(g, (3, 2, 0, 1))
 
         @pl.when(jnp.logical_and(r >= 0, r < total))
         def _():
-            g = in_turn(r)
-            send_sum(g, 3, inward, True)
+            send_sum(in_turn(r), 3, inward, True)
+
+        @pl.when(jnp.logical_and(r >= LAG_OUT, r < total + LAG_OUT))
+        def _():
+            send_sum(in_turn(r - LAG_OUT), 0, outward, True)
+
+        @pl.when(jnp.logical_and(r >= LAG_NEAR, r < total + LAG_NEAR))
+        def _():
+            g = in_turn(r - LAG_NEAR)
             send_sum(g, 2, inward, True)
             own_sum[g] = pair_sum(g, z)
-
-        @pl.when(r >= LAG_OUT)
-        def _():
-            send_sum(in_turn(r - LAG_OUT), 0, outward, True)
 
         @pl.when(r >= LAG_FINAL)
         def _():
@@ -456,13 +499,22 @@
             if kind == DOWN:
                 make_cots(p)
             middle_reduce(t - LAG)
-        input_terms(p)
+        turn_cots(p)
         return carry
 
     def middle_rest(r, carry):
         middle_reduce(r)
-
-        @pl.when(r == total - INPUT_TURN)
+        turn = r - (total - LAG)
+
+        @pl.when(turn < 2)
+        def _():
+            input_base(turn)
+
+        @pl.when(turn == 2)
+        def _():
+            input_last()
+
+        @pl.when(turn == INPUT_TURN)
         def _():
             input_relay()
 
@@ -568,6 +620,8 @@
             pltpu.VMEM((pieces, n, height, rows), bf16),
             pltpu.VMEM((3, height, count), f32),
             pltpu.VMEM((pieces, height, count), bf16),
+            pltpu.VMEM((2 * PARTS, count, height), bf16),
+            pltpu.VMEM((pieces, nz, height, rows), f32),
             pltpu.VMEM((pieces, nz, height, rows), bf16),
             pltpu.VMEM((pieces, nz, height, rows), bf16),
             pltpu.VMEM((pieces, nz, height, rows), bf16),

time: 115 us -> 110 us (0.957)
  Pallas kernels: 114 us -> 109 us
    pallas_call x1, Pallas kernels: 112 us -> 108 us  [fused_shards(): pl.pallas_call(functools.partial(kernel, n, n_tp, PARTS), out_shape=(pltp...]
where the time goes in v3:
time: 110 us
  Pallas kernels  109 us (99%)
    pallas_call x1, Pallas kernels, fused_shards(): pl.pallas_call(functools.partial(kernel, n, n_tp, PARTS), out_shape=(pltp...  108 us

profile of v3, /device:TPU:0, one launch (start us, length us, event | category | flops | bytes accessed | tf_op | source)
XLA Modules:
  0.0 109.9 jit_solution(5623004300194512100)
XLA Ops:
  0.6 107.6 %shard_map.84 = (bf16[512,512]{1,0:T(8,128)(2,1)S(1)}, f32[12,176,256]{2,1,0:T(8,128)S(1)}) custom-call(bf16[512,2048]{1,0:T(8,128)(2,1)} %tok.1, bf16[512,2048]{1,0:T(8,128)(2,1)} %cot.1, bf16[704,256]{1,0:T(8,128)(2,1)} %bitcast.6, bf16[704,256]{1,0:T(8,128)(2,1)} %bitcast.7, bf16[704,256]{1,0:T(8,128)(2,1)} %bitcast.8), custom_call_target="tpu_custom_call" | custom-call | tf_op jit(solution)/shard_map/pallas_call | solution.py:613
  108.2 1.6 %shard_map.85 = (bf16[512,512]{1,0:T(8,128)(2,1)}, f32[704,256]{1,0:T(8,128)}, f32[704,256]{1,0:T(8,128)}, f32[704,256]{1,0:T(8,128)}) custom-call(bf16[512,512]{1,0:T(8,128)(2,1)S(1)} %get-tuple-element.10.ig, f32[12,176,256]{2,1,0:T(8,128)S(1)} %get-tuple-element.11.sums), custom_call_target="tpu_custom_call" | custom-call | tf_op jit(solution)/shard_map/pallas_call | solution.py:647

commit v4 on v3

--- a/solution.py
+++ b/solution.py
@@ -73,9 +73,10 @@
 LAG = 7
 VMEM_BYTES = 60 * 1024 * 1024
 DELIVER_BYTES = 1024 * 1024
-LAG_OUT, LAG_NEAR, LAG_FINAL = 2, 1, 5
+LAG_OUT, LAG_NEAR, LAG_FINAL = 3, 1, 5
 INPUT_TURN = 5
-OWN_IN, OWN_OUT = 2, 3
+OWN_IN, OWN_OUT = 1, 1
+FIRST_IN, FIRST_OUT = 2, 3
 RELAY_IN, RELAY_OUT = 2, 1
 GATE, UP, DOWN = 0, 1, 2
 RIGHT, LEFT, SIBLING = 0, 1, 2
@@ -114,7 +115,7 @@
         pltpu.make_async_copy(tok, x.at[0], local_sem.at[total]),
         pltpu.make_async_copy(cot, x.at[1], local_sem.at[total + 1]),
     ]
-    for load in loads:
+    for load in loads[:total]:
         load.start()
 
     has_left, has_right = z > 0, z < nz - 1
@@ -333,6 +334,23 @@
 
         lax.fori_loop(0, n_tp, body, 0)
 
+    def drain_early(g, carry):
+        for q in range(nz):
+            gather_copy(g, q, SIBLING).wait_send()
+            sibling_copy(g, chip_at(q)).wait_send()
+        return carry
+
+    def end_drain(g, carry):
+        gather_copy(g, 0, inward).wait_send()
+        return drain_early(g, carry)
+
+    def middle_drain(g, carry):
+        for q in (1, 2, 3):
+            gather_copy(g, q, outward).wait_send()
+        for q in (0, 1):
+            gather_copy(g, q, inward).wait_send()
+        return drain_early(g, carry)
+
     def end_gather(t, kind):
         gather_wait(t, 1, c)
         gather_copy(t, 1, SIBLING).start()
@@ -416,7 +434,7 @@
             gather_copy(t, 0, inward).start()
             gather_copy(t, 0, SIBLING).start()
 
-        @pl.when(t + OWN_IN < total)
+        @pl.when(jnp.logical_and(t + OWN_IN >= FIRST_IN, t + OWN_IN < total))
         def _():
             gather_copy(t + OWN_IN, 1, inward).start()
 
@@ -434,7 +452,7 @@
             gather_copy(t, 3, outward).start()
             gather_copy(t, 3, SIBLING).start()
 
-        @pl.when(t + OWN_OUT < total)
+        @pl.when(jnp.logical_and(t + OWN_OUT >= FIRST_OUT, t + OWN_OUT < total))
         def _():
             gather_copy(t + OWN_OUT, 1, outward).start()
 
@@ -514,6 +532,10 @@
         def _():
             input_last()
 
+        @pl.when(jnp.logical_and(turn > 2, turn < 8))
+        def _():
+            lax.fori_loop((turn - 3) * 2, (turn - 2) * 2, middle_drain, 0)
+
         @pl.when(turn == INPUT_TURN)
         def _():
             input_relay()
@@ -521,6 +543,9 @@
         return carry
 
     for t in range(total):
+        if t == FIRST_OUT:
+            for load in loads[total:]:
+                load.start()
         loads[t].wait()
         gather_copy(t, jnp.where(is_end, 0, 1), SIBLING).start()
 
@@ -528,23 +553,24 @@
         def _():
             gather_copy(t, 0, inward).start()
 
-        if t < OWN_OUT:
+        if t < FIRST_OUT:
             @pl.when(jnp.logical_not(is_end))
             def _():
                 gather_copy(t, 1, outward).start()
 
-        if t < OWN_IN:
+        if t < FIRST_IN:
             @pl.when(jnp.logical_not(is_end))
             def _():
                 gather_copy(t, 1, inward).start()
 
-    loads[total].wait()
-    loads[total + 1].wait()
+    for load in loads[total:]:
+        load.wait()
 
     @pl.when(is_end)
     def _():
         lax.fori_loop(0, parts, end_part, 0)
         input_relay()
+        lax.fori_loop(0, total, end_drain, 0)
         lax.fori_loop(0, total, final, 0)
 
     @pl.when(jnp.logical_not(is_end))
@@ -556,6 +582,7 @@
             relay_far(t)
         lax.fori_loop(0, parts, middle_part, 0)
         lax.fori_loop(total - LAG, total + LAG_OUT, middle_rest, 0)
+        lax.fori_loop(total - 2, total, middle_drain, 0)
         lax.fori_loop(total + LAG_OUT - LAG_FINAL, total, middle_final, 0)
 
     for s in range(2):
@@ -566,35 +593,19 @@
             value = value + ig_in[k].astype(jnp.float32)
         ig_out[half_rows(s), :] = value.astype(ig_out.dtype)
 
-    def drain(g, carry):
-        for chip in range(nz):
-            gather_copy(g, chip, SIBLING).wait_send()
-            sibling_copy(g, chip).wait_send()
+    def drain_lines(r, carry):
+        g = in_turn(r)
+        for q in range(nz):
+            chip = chip_at(q)
 
             @pl.when(chip != z)
             def _():
                 way = jnp.where(chip > z, RIGHT, LEFT)
                 line_copy(g, way, chip).wait_send()
 
-            @pl.when(jnp.logical_and(has_right, chip <= z))
-            def _():
-                absolute_copy(g, chip, RIGHT).wait_send()
-
-            @pl.when(jnp.logical_and(has_left, chip >= z))
-            def _():
-                absolute_copy(g, chip, LEFT).wait_send()
-
         return carry
 
-    def absolute_copy(t, chip, way):
-        slot = 2 * chip + c
-        return pltpu.make_async_remote_copy(
-            src_ref=w_all.at[t, slot], dst_ref=w_all.at[t, slot],
-            send_sem=ag_send.at[t, way, chip], recv_sem=ag_recv.at[t, slot],
-            device_id={"fs": line_device(way)}, device_id_type=MESH,
-        )
-
-    lax.fori_loop(0, total, drain, 0)
+    lax.fori_loop(0, total, drain_lines, 0)
     for s in range(2):
         for copy in (corner_copy, direct_copy, relay_copy):
             copy(s).wait_send()

time: 110 us -> 108 us (0.982)
  Pallas kernels: 109 us -> 107 us
    pallas_call x1, Pallas kernels: 108 us -> 106 us  [fused_shards(): pl.pallas_call(functools.partial(kernel, n, n_tp, PARTS), out_shape=(pltp...]
where the time goes in v4:
time: 108 us
  Pallas kernels  107 us (99%)
    pallas_call x1, Pallas kernels, fused_shards(): pl.pallas_call(functools.partial(kernel, n, n_tp, PARTS), out_shape=(pltp...  106 us

profile of v4, /device:TPU:0, one launch (start us, length us, event | category | flops | bytes accessed | tf_op | source)
XLA Modules:
  0.0 108.1 jit_solution(14441802367316724946)
XLA Ops:
  0.6 105.9 %shard_map.84 = (bf16[512,512]{1,0:T(8,128)(2,1)S(1)}, f32[12,176,256]{2,1,0:T(8,128)S(1)}) custom-call(bf16[512,2048]{1,0:T(8,128)(2,1)} %tok.1, bf16[512,2048]{1,0:T(8,128)(2,1)} %cot.1, bf16[704,256]{1,0:T(8,128)(2,1)} %bitcast.6, bf16[704,256]{1,0:T(8,128)(2,1)} %bitcast.7, bf16[704,256]{1,0:T(8,128)(2,1)} %bitcast.8), custom_call_target="tpu_custom_call" | custom-call | tf_op jit(solution)/shard_map/pallas_call | solution.py:624
  106.5 1.6 %shard_map.85 = (bf16[512,512]{1,0:T(8,128)(2,1)}, f32[704,256]{1,0:T(8,128)}, f32[704,256]{1,0:T(8,128)}, f32[704,256]{1,0:T(8,128)}) custom-call(bf16[512,512]{1,0:T(8,128)(2,1)S(1)} %get-tuple-element.10.ig, f32[12,176,256]{2,1,0:T(8,128)S(1)} %get-tuple-element.11.sums), custom_call_target="tpu_custom_call" | custom-call | tf_op jit(solution)/shard_map/pallas_call | solution.py:658

commit v5 on v4

--- a/solution.py
+++ b/solution.py
@@ -73,7 +73,7 @@
 LAG = 7
 VMEM_BYTES = 60 * 1024 * 1024
 DELIVER_BYTES = 1024 * 1024
-LAG_OUT, LAG_NEAR, LAG_FINAL = 3, 1, 5
+LAG_OUT, LAG_NEAR, LAG_FINAL = 3, 2, 5
 INPUT_TURN = 5
 OWN_IN, OWN_OUT = 1, 1
 FIRST_IN, FIRST_OUT = 2, 3

time: 108 us -> 108 us (level)
  no operation moved by 1% of the time
where the time goes in v5:
time: 108 us
  Pallas kernels  107 us (99%)
    pallas_call x1, Pallas kernels, fused_shards(): pl.pallas_call(functools.partial(kernel, n, n_tp, PARTS), out_shape=(pltp...  106 us

profile of v5, /device:TPU:0, one launch (start us, length us, event | category | flops | bytes accessed | tf_op | source)
XLA Modules:
  0.0 108.1 jit_solution(5623079453995651414)
XLA Ops:
  0.6 105.9 %shard_map.84 = (bf16[512,512]{1,0:T(8,128)(2,1)S(1)}, f32[12,176,256]{2,1,0:T(8,128)S(1)}) custom-call(bf16[512,2048]{1,0:T(8,128)(2,1)} %tok.1, bf16[512,2048]{1,0:T(8,128)(2,1)} %cot.1, bf16[704,256]{1,0:T(8,128)(2,1)} %bitcast.6, bf16[704,256]{1,0:T(8,128)(2,1)} %bitcast.7, bf16[704,256]{1,0:T(8,128)(2,1)} %bitcast.8), custom_call_target="tpu_custom_call" | custom-call | tf_op jit(solution)/shard_map/pallas_call | solution.py:624
  106.5 1.6 %shard_map.85 = (bf16[512,512]{1,0:T(8,128)(2,1)}, f32[704,256]{1,0:T(8,128)}, f32[704,256]{1,0:T(8,128)}, f32[704,256]{1,0:T(8,128)}) custom-call(bf16[512,512]{1,0:T(8,128)(2,1)S(1)} %get-tuple-element.10.ig, f32[12,176,256]{2,1,0:T(8,128)S(1)} %get-tuple-element.11.sums), custom_call_target="tpu_custom_call" | custom-call | tf_op jit(solution)/shard_map/pallas_call | solution.py:658
